TPU v7x, 32 devices: a whole 2x2x4 slice. The times are simulated.
32 devices in a mesh: sp: 8 (over z, x), tp: 4 (over y, core).
Axes of the slice: x: 2, y: 2, z: 4, core: 2. Of those that a mesh axis runs over, the one named last changes fastest.
Arguments:
- residual_in: bfloat16 [2048, 2048], P(('sp', 'tp')), may hold values from -0.119628906 to 0.119628906
- queries: bfloat16 [2048, 2048], P('sp', 'tp'), may hold values from -6 to 6
- keys_raw: bfloat16 [2048, 512], P('sp', 'tp'), may hold values from -6 to 6
- values_raw: bfloat16 [2048, 512], P('sp', 'tp'), may hold values from -6 to 6
- query_gain: float32 [128], replicated, may hold values from 0.28 to 7
- key_gain: float32 [128], replicated, may hold values from 0.28 to 7
- out_weight: bfloat16 [2048, 2048], P('tp'), may hold values from -0.125 to 0.125
- norm_gain: float32 [2048], replicated, may hold values from 0.1 to 1.9
- gate_weight: bfloat16 [2048, 5632], P('sp', 'tp'), may hold values from -0.125 to 0.125
- up_weight: bfloat16 [2048, 5632], P('sp', 'tp'), may hold values from -0.125 to 0.125
- down_weight: bfloat16 [5632, 2048], P('tp', 'sp'), may hold values from -0.078125 to 0.078125
Outputs:
- residual_out: bfloat16 [2048, 2048], P(('sp', 'tp'))
All inputs are finite; a program needn't handle non-finite values.
Results may differ from a plain program's by a relative error of at most 0.024.
The roundings to bfloat16 on the way count: a program that leaves them out, or rounds other values in their place, can miss the bound.
Values may be sent and summed in bfloat16 or wider, within the bound.
A program may use at most 128 MiB of HBM per device.

v0:
```python
import jax
import jax.numpy as jnp
from jax import lax
from jax.sharding import PartitionSpec as P

GRID_W = 64
EPS = 1e-06
THETA = 10000.0


def turn_half(part, angles):
    quarter = part.shape[-1] // 2
    cosine = jnp.cos(angles)[:, None, :]
    sine = jnp.sin(angles)[:, None, :]
    first = part[..., :quarter]
    second = part[..., quarter:]
    return part * cosine + jnp.concatenate([-second, first], axis=-1) * sine


def prepare_heads(raw, gain, positions, heads):
    count = raw.shape[0]
    head_dim = gain.shape[0]
    half = head_dim // 2
    vec = raw.astype(jnp.float32).reshape(count, heads, head_dim)
    vec = vec * lax.rsqrt(jnp.mean(vec * vec, axis=-1, keepdims=True) + EPS) * gain
    freqs = THETA ** (-jnp.arange(0, half, 2, dtype=jnp.float32) / half)
    row_ang = (positions // GRID_W).astype(jnp.float32)[:, None] * freqs
    col_ang = (positions % GRID_W).astype(jnp.float32)[:, None] * freqs
    row_ang = jnp.concatenate([row_ang, row_ang], axis=-1)
    col_ang = jnp.concatenate([col_ang, col_ang], axis=-1)
    turned = jnp.concatenate(
        [turn_half(vec[..., :half], row_ang), turn_half(vec[..., half:], col_ang)], axis=-1
    )
    return turned.astype(jnp.bfloat16)


def per_device(
    residual_in,
    queries,
    keys_raw,
    values_raw,
    query_gain,
    key_gain,
    out_weight,
    norm_gain,
    gate_weight,
    up_weight,
    down_weight,
):
    tok = queries.shape[0]
    head_dim = query_gain.shape[0]
    local_heads = queries.shape[1] // head_dim
    local_kv = keys_raw.shape[1] // head_dim
    group = local_heads // local_kv
    gate_full, up_full = (
        lax.all_gather(gate_weight, "sp", axis=0, tiled=True),
        lax.all_gather(up_weight, "sp", axis=0, tiled=True),
    )
    down_full = lax.all_gather(down_weight, "sp", axis=1, tiled=True)
    positions = lax.axis_index("sp") * tok + jnp.arange(tok, dtype=jnp.int32)
    q_rot = prepare_heads(queries, query_gain, positions, local_heads).reshape(
        tok, local_kv, group, head_dim
    )
    k_rot = prepare_heads(keys_raw, key_gain, positions, local_kv)
    vals = values_raw.reshape(tok, local_kv, head_dim)
    start_state = (
        jnp.full((tok, local_kv, group), -jnp.inf, jnp.float32),
        jnp.zeros((tok, local_kv, group), jnp.float32),
        jnp.zeros((tok, local_kv, group, head_dim), jnp.float32),
    )
    carry = start_state
    k_piece = lax.all_gather(k_rot, "sp", axis=0, tiled=True)
    v_piece = lax.all_gather(vals, "sp", axis=0, tiled=True)
    length = k_piece.shape[0]
    shards = length // tok
    per_step = max(1, 2048 // tok)
    factor = max((d for d in range(1, shards + 1) if shards % d == 0 and d <= per_step))
    span = factor * tok
    k_blocks = k_piece.reshape(length // span, span, local_kv, head_dim)
    v_blocks = v_piece.reshape(length // span, span, local_kv, head_dim)

    def step(state, blocks):
        top, total, summed = state
        k_blk, v_blk = blocks
        scores = jnp.einsum(
            "qkgd,skd->qkgs", q_rot, k_blk, preferred_element_type=jnp.float32
        ) * head_dim ** (-0.5)
        new_top = jnp.maximum(top, jnp.max(scores, axis=-1))
        shrink = jnp.exp(top - new_top)
        expo = jnp.exp(scores - new_top[..., None])
        total = total * shrink + jnp.sum(expo, axis=-1)
        summed = summed * shrink[..., None] + jnp.einsum(
            "qkgs,skd->qkgd", expo.astype(jnp.bfloat16), v_blk, preferred_element_type=jnp.float32
        )
        return ((new_top, total, summed), None)

    carry, _ = lax.scan(step, carry, (k_blocks, v_blocks))
    top, total, summed = carry
    attended = (summed / total[..., None]).astype(jnp.bfloat16).reshape(tok, local_heads * head_dim)
    projected = lax.psum_scatter(
        jnp.dot(attended, out_weight, preferred_element_type=jnp.float32).astype(jnp.bfloat16),
        "tp",
        scatter_dimension=0,
        tiled=True,
    ).astype(jnp.float32)
    mixed = (residual_in.astype(jnp.float32) + projected).astype(jnp.bfloat16)
    mixed_f = mixed.astype(jnp.float32)
    normed = (
        mixed_f * lax.rsqrt(jnp.mean(mixed_f * mixed_f, axis=-1, keepdims=True) + EPS) * norm_gain
    ).astype(jnp.bfloat16)
    whole_rows = lax.all_gather(normed, "tp", axis=0, tiled=True)
    gate = jnp.dot(whole_rows, gate_full, preferred_element_type=jnp.float32)
    up_val = jnp.dot(whole_rows, up_full, preferred_element_type=jnp.float32)
    hidden = (jax.nn.silu(gate) * up_val).astype(jnp.bfloat16)
    terms = jnp.dot(hidden, down_full, preferred_element_type=jnp.float32)
    fed = lax.psum_scatter(
        terms.astype(jnp.bfloat16), "tp", scatter_dimension=0, tiled=True
    ).astype(jnp.float32)
    return (mixed_f + 0.5 * fed).astype(jnp.bfloat16)


def solution(mesh):
    placed = (
        P(("sp", "tp"), None),
        P("sp", "tp"),
        P("sp", "tp"),
        P("sp", "tp"),
        P(),
        P(),
        P("tp", None),
        P(),
        P("sp", "tp"),
        P("sp", "tp"),
        P("tp", "sp"),
    )
    return jax.shard_map(
        per_device, mesh=mesh, in_specs=placed, out_specs=P(("sp", "tp"), None), check_vma=False
    )
```

profile of v0, /device:TPU:0, one launch (start us, length us, event | category | flops | bytes accessed | tf_op | source)
XLA Modules:
  0.0 460.9 jit_solution(13443270139341550448)
XLA Ops:
  6.5 0.0 reduce-scatter.3.cloned.1.call-start
  6.6 1.1 fusion.33
  7.7 0.9 fusion.35
  8.6 0.2 slice_negate_fusion.3
  8.8 0.8 broadcast_multiply_fusion.1
  9.6 1.2 fusion.39
  10.8 0.1 pad_maximum_fusion.4
  10.9 33.0 %all_gather.18 = bf16[2048,1,128]{2,0,1:T(8,128)(2,1)S(1)} all-gather(bf16[256,1,128]{2,0,1:T(8,128)(2,1)S(1)} %pad_maximum_fusion.4), channel_id=1, replica_groups=mesh['sp'=8,'tp'=4] {'sp'}, dimensions={0}, use_global_device_ids=true | all-gather | bytes 589824 | tf_op jit(solution)/shard_map/all_gather | solution.py:72
  43.9 1.1 copy.14
  45.0 0.1 multiply_reduce_fusion
  45.1 0.1 copy.15
  45.2 0.9 multiply_multiply_fusion
  46.1 0.5 slice_negate_fusion.1
  46.6 1.5 fusion.43
  48.1 0.5 fusion.41
  48.7 0.5 fusion.26
  49.1 1.3 bitcast_reduce_fusion
  50.5 0.0 copy-start.4
  50.5 3.2 copy-done.1
  53.7 1.4 fusion.1
  55.1 0.0 copy-done.4
  55.1 0.1 copy.16
  55.2 31.3 %all-gather = bf16[2048,128]{0,1:T(8,128)(2,1)S(1)} all-gather(bf16[256,128]{0,1:T(8,128)(2,1)S(1)} %copy.16), channel_id=2, replica_groups=mesh['sp'=8,'tp'=4] {'sp'}, dimensions={0}, use_global_device_ids=true | all-gather | bytes 589824 | tf_op jit(solution)/shard_map/all_gather | solution.py:73
  86.5 5.1 %fusion.16 = bf16[1,128,256,4]{2,1,3,0:T(8,128)(2,1)S(1)} fusion(f32[2048,256,4]{1,0,2:T(8,128)} %copy-done.1, f32[256,4]{0,1:T(4,128)S(1)} %get-tuple-element.50, bf16[2048,128]{0,1:T(8,128)(2,1)S(1)} %all-gather, f32[256,4]{0,1:T(4,128)S(1)} %get-tuple-element.43, f32[256,4]{0,1:T(4,128)S(1)} %get-tuple-element.42), kind=kOutput, calls=%fused_computation.14 | convolution fusion | flops 543555584 | bytes 9187328 | tf_op jit(solution)/shard_map/while/body/eval_jaxpr/qkgs,skd->qkgd/dot_general | solution.py:92
  91.6 1.7 convolution_convert_fusion
  93.3 0.0 reduce-scatter.3.cloned.1.call-update
  93.3 0.0 all-gather.6.cloned.1.call-start
  93.4 26.1 %reduce-scatter.3.cloned.1.call-done = bf16[64,2048]{1,0:T(8,128)(2,1)} async-done(((bf16[256,2048]{1,0:T(8,128)(2,1)}), bf16[64,2048]{1,0:T(8,128)(2,1)}) %reduce-scatter.3.cloned.1.call-update) | async-done | bytes 262160 | tf_op jit(solution)/shard_map/reduce_scatter | solution.py:100
  119.4 1.1 fusion.19
  120.6 0.0 copy-done.5
  120.6 1.8 fusion.21
  122.4 0.0 all-gather.6.cloned.1.call-update
  122.4 0.0 all-gather.8.cloned.1.call-start
  122.5 0.7 all-gather.8.cloned.1.call-update
  123.1 0.0 all-gather.10.cloned.1.call-start
  123.2 0.5 all-gather.10.cloned.1.call-update
  123.7 0.0 all-gather.12.cloned.1.call-start
  123.8 0.5 all-gather.12.cloned.1.call-update
  124.3 0.2 reduce-scatter.5.cloned.1.call-start
  124.5 14.7 %all-gather.6.cloned.1.call-done = bf16[256,2048]{1,0:T(8,128)(2,1)} async-done(((bf16[64,2048]{1,0:T(8,128)(2,1)}), bf16[256,2048]{1,0:T(8,128)(2,1)}) %all-gather.6.cloned.1.call-update) | async-done | bytes 1048592 | tf_op jit(solution)/shard_map/all_gather | solution.py:111
  139.3 94.5 %all-gather.8.cloned.1.call-done = bf16[2048,1408]{1,0:T(8,128)(2,1)} async-done(((bf16[256,1408]{1,0:T(8,128)(2,1)}), bf16[2048,1408]{1,0:T(8,128)(2,1)}) %all-gather.8.cloned.1.call-update) | async-done | bytes 5767184 | tf_op jit(solution)/shard_map/all_gather | solution.py:56
  233.8 5.9 %fusion.53 = f32[256,1408]{1,0:T(8,128)} fusion(bf16[256,2048]{1,0:T(8,128)(2,1)} %all-gather.6.cloned.1.call-done, bf16[2048,1408]{1,0:T(8,128)(2,1)} %all-gather.8.cloned.1.call-done), kind=kOutput, calls=%fused_computation.88 | convolution fusion | flops 1476395008 | bytes 8257536 | tf_op jit(solution)/shard_map/dot_general | solution.py:112
  239.7 86.7 %all-gather.10.cloned.1.call-done = bf16[2048,1408]{1,0:T(8,128)(2,1)} async-done(((bf16[256,1408]{1,0:T(8,128)(2,1)}), bf16[2048,1408]{1,0:T(8,128)(2,1)}) %all-gather.10.cloned.1.call-update) | async-done | bytes 5767184 | tf_op jit(solution)/shard_map/all_gather | solution.py:57
  326.3 93.2 %all-gather.12.cloned.1.call-done = bf16[1408,2048]{1,0:T(8,128)(2,1)} async-done(((bf16[1408,256]{1,0:T(8,128)(2,1)}), bf16[1408,2048]{1,0:T(8,128)(2,1)}) %all-gather.12.cloned.1.call-update) | async-done | bytes 5767184 | tf_op jit(solution)/shard_map/all_gather | solution.py:59
  419.6 9.5 %convolution_convert_fusion.1 = bf16[256,2048]{1,0:T(8,128)(2,1)} fusion(bf16[1408,2048]{1,0:T(8,128)(2,1)} %all-gather.12.cloned.1.call-done, bf16[256,2048]{1,0:T(8,128)(2,1)} %all-gather.6.cloned.1.call-done, bf16[2048,1408]{1,0:T(8,128)(2,1)} %all-gather.10.cloned.1.call-done, f32[256,1408]{1,0:T(8,128)} %fusion.53), kind=kOutput, calls=%fused_computation.10 | convolution fusion | flops 2955476992 | bytes 15073280 | tf_op jit(solution)/shard_map/dot_general | solution.py:115
  429.1 0.0 reduce-scatter.5.cloned.1.call-update
  429.1 23.1 %reduce-scatter.5.cloned.1.call-done = bf16[64,2048]{1,0:T(8,128)(2,1)} async-done(((bf16[256,2048]{1,0:T(8,128)(2,1)}), bf16[64,2048]{1,0:T(8,128)(2,1)}) %reduce-scatter.5.cloned.1.call-update) | async-done | bytes 262160 | tf_op jit(solution)/shard_map/reduce_scatter | solution.py:116
  452.3 1.8 fusion.22
  (14 shorter events, 0.1 us)
Async XLA Ops:
  6.5 85.0 %copy-start = (bf16[512,2048]{1,0:T(8,128)(2,1)S(1)}, bf16[512,2048]{1,0:T(8,128)(2,1)}, u32[]{:S(2)}) copy-start(bf16[512,2048]{1,0:T(8,128)(2,1)} %param.17) | copy-start | bytes 6291460
  6.5 112.9 %reduce-scatter.3.cloned.1.call-start = ((), (), s32[]{:S(2)}) async-start(), calls=%async_computation.2 | async-start | bytes 1310720 | tf_op jit(solution)/shard_map/reduce_scatter | solution.py:100
  50.5 3.2 copy-start.1
  50.5 4.6 %copy-start.4 = (bf16[256,128]{1,0:T(8,128)(2,1)S(1)}, bf16[256,128]{1,0:T(8,128)(2,1)}, u32[]{:S(2)}) copy-start(bf16[256,128]{1,0:T(8,128)(2,1)} %param.14) | copy-start | bytes 196612
  86.5 32.9 %copy-start.2 = (bf16[64,2048]{1,0:T(8,128)(2,1)S(1)}, bf16[64,2048]{1,0:T(8,128)(2,1)}, u32[]{:S(2)}) copy-start(bf16[64,2048]{1,0:T(8,128)(2,1)} %param.11) | copy-start | bytes 786436
  86.5 34.1 %copy-start.5 = (f32[2048]{0:T(1024)S(1)}, f32[2048]{0:T(1024)}, u32[]{:S(2)}) copy-start(f32[2048]{0:T(1024)} %param.18) | copy-start | bytes 24580
  93.3 45.9 %all-gather.6.cloned.1.call-start = ((), (), s32[]{:S(2)}) async-start(), calls=%async_computation.3 | async-start | bytes 1310720 | tf_op jit(solution)/shard_map/all_gather | solution.py:111
  122.4 111.4 %all-gather.8.cloned.1.call-start = ((), (), s32[]{:S(2)}) async-start(), calls=%async_computation.4 | async-start | bytes 6488064 | tf_op jit(solution)/shard_map/all_gather | solution.py:56
  123.1 203.2 %all-gather.10.cloned.1.call-start = ((), (), s32[]{:S(2)}) async-start(), calls=%async_computation.5 | async-start | bytes 6488064 | tf_op jit(solution)/shard_map/all_gather | solution.py:57
  123.7 295.9 %all-gather.12.cloned.1.call-start = ((), (), s32[]{:S(2)}) async-start(), calls=%async_computation.6 | async-start | bytes 6488064 | tf_op jit(solution)/shard_map/all_gather | solution.py:59
  124.3 327.9 %reduce-scatter.5.cloned.1.call-start = ((), (), s32[]{:S(2)}) async-start(), calls=%async_computation.7 | async-start | bytes 1310720 | tf_op jit(solution)/shard_map/reduce_scatter | solution.py:116
  239.7 212.6 %copy-start.3 = (bf16[64,2048]{1,0:T(8,128)(2,1)S(1)}, bf16[64,2048]{1,0:T(8,128)(2,1)}, u32[]{:S(2)}) copy-start(bf16[64,2048]{1,0:T(8,128)(2,1)} %reduce-scatter.3.cloned.1.call-done) | copy-start | bytes 786436
Sparse Core Ops, SparseCore 0:
  93.4 25.9 reduce-scatter.2
  122.5 16.6 all-gather.5
  141.4 92.2 all-gather.7
  235.8 90.4 all-gather.9
  328.2 91.2 all-gather.11
  429.2 22.9 reduce-scatter.4
where the time goes:
time: 461 us
  waiting for transfers between devices  340 us (74%)
  blocking collectives  64.3 us (14%)
  matrix products  23.5 us (5%)
  other arithmetic  14.3 us (3%)
  between operations  13.6 us (3%)
    all_gather x1, waiting for transfers between devices, per_device(): lax.all_gather(gate_weight, 'sp', axis=0, tiled=True)  94.5 us
    all_gather x1, waiting for transfers between devices, per_device(): down_full = lax.all_gather(down_weight, 'sp', axis=1, tiled=True)  93.2 us
    all_gather x1, waiting for transfers between devices, per_device(): lax.all_gather(up_weight, 'sp', axis=0, tiled=True)  86.7 us
    all_gather x1, blocking collectives, per_device(): k_piece = lax.all_gather(k_rot, 'sp', axis=0, tiled=True)  33 us
    all_gather x1, blocking collectives, per_device(): v_piece = lax.all_gather(vals, 'sp', axis=0, tiled=True)  31.3 us
    reduce_scatter x1, waiting for transfers between devices, per_device(): lax.psum_scatter(jnp.dot(attended, out_weight, preferred_element_type=jnp...  26.1 us
    reduce_scatter x1, waiting for transfers between devices, per_device(): lax.psum_scatter(terms.astype(jnp.bfloat16), 'tp', scatter_dimension=0, t...  23.1 us
    all_gather x1, waiting for transfers between devices, per_device(): whole_rows = lax.all_gather(normed, 'tp', axis=0, tiled=True)  14.7 us
  transfers between devices with their start and end apart: 6, of which 6 were waited for; matrix products, arithmetic and copies ran while one was open for 1% of the time, Pallas kernels for 0%

commit v1 on v0

--- a/solution.py
+++ b/solution.py
@@ -56,7 +56,8 @@
         lax.all_gather(gate_weight, "sp", axis=0, tiled=True),
         lax.all_gather(up_weight, "sp", axis=0, tiled=True),
     )
-    down_full = lax.all_gather(down_weight, "sp", axis=1, tiled=True)
+    pieces = lax.all_gather(down_weight, "sp")
+    down_full = jnp.concatenate(pieces, axis=1)
     positions = lax.axis_index("sp") * tok + jnp.arange(tok, dtype=jnp.int32)
     q_rot = prepare_heads(queries, query_gain, positions, local_heads).reshape(
         tok, local_kv, group, head_dim

time: 461 us -> 436 us (0.946)
  waiting for transfers between devices: 340 us -> 304 us
  local copies, waits for them, and re-layouts: 4.56 us -> 12.9 us
    all_gather x1, waiting for transfers between devices: 93.2 us -> 65.4 us  [per_device(): pieces = lax.all_gather(down_weight, 'sp')]
    reshape x0 -> x1, local copies, waits for them, and re-layouts: none -> 8.32 us  [per_device(): down_full = jnp.concatenate(pieces, axis=1)]
    all_gather x1, waiting for transfers between devices: 14.7 us -> 7.86 us  [per_device(): whole_rows = lax.all_gather(normed, 'tp', axis=0, tiled=True)]
  transfers between devices with their start and end apart: 6 -> 6, of which waited for: 6 -> 6; matrix products, arithmetic and copies ran while one was open for 1% -> 4% of each run, Pallas kernels for 0% -> 0%
where the time goes in v1:
time: 436 us; the launch traced here: 435 us
  waiting for transfers between devices  304 us (70%)
  blocking collectives  64.3 us (15%)
  matrix products  23.5 us (5%)
  between operations  15.2 us (3%)
  other arithmetic  14.3 us (3%)
  local copies, waits for them, and re-layouts  12.9 us (3%)
    all_gather x1, waiting for transfers between devices, per_device(): lax.all_gather(gate_weight, 'sp', axis=0, tiled=True)  94.2 us
    all_gather x1, waiting for transfers between devices, per_device(): lax.all_gather(up_weight, 'sp', axis=0, tiled=True)  86.6 us
    all_gather x1, waiting for transfers between devices, per_device(): pieces = lax.all_gather(down_weight, 'sp')  65.4 us
    all_gather x1, blocking collectives, per_device(): k_piece = lax.all_gather(k_rot, 'sp', axis=0, tiled=True)  33 us
    all_gather x1, blocking collectives, per_device(): v_piece = lax.all_gather(vals, 'sp', axis=0, tiled=True)  31.3 us
    reduce_scatter x1, waiting for transfers between devices, per_device(): lax.psum_scatter(jnp.dot(attended, out_weight, preferred_element_type=jnp...  25.5 us
    reduce_scatter x1, waiting for transfers between devices, per_device(): lax.psum_scatter(terms.astype(jnp.bfloat16), 'tp', scatter_dimension=0, t...  23.1 us
    dot_general x1, matrix products, per_device(): terms = jnp.dot(hidden, down_full, preferred_element_type=jnp.float32)  9.5 us
  transfers between devices with their start and end apart: 6, of which 6 were waited for; matrix products, arithmetic and copies ran while one was open for 4% of the time, Pallas kernels for 0%

profile of v1, /device:TPU:0, one launch (start us, length us, event | category | flops | bytes accessed | tf_op | source)
XLA Modules:
  0.0 435.1 jit_solution(1341825198377460762)
XLA Ops:
  7.4 0.0 copy-start
  7.4 0.0 reduce-scatter.3.cloned.1.call-start
  7.4 1.1 fusion.33
  8.5 0.9 fusion.35
  9.5 0.2 slice_negate_fusion.3
  9.6 0.8 broadcast_multiply_fusion.1
  10.4 1.2 fusion.39
  11.6 0.1 pad_maximum_fusion.4
  11.7 33.0 %all_gather.21 = bf16[2048,1,128]{2,0,1:T(8,128)(2,1)S(1)} all-gather(bf16[256,1,128]{2,0,1:T(8,128)(2,1)S(1)} %pad_maximum_fusion.4), channel_id=1, replica_groups=mesh['sp'=8,'tp'=4] {'sp'}, dimensions={0}, use_global_device_ids=true | all-gather | bytes 589824 | tf_op jit(solution)/shard_map/all_gather | solution.py:73
  44.8 1.1 copy.18
  45.8 0.1 multiply_reduce_fusion
  45.9 0.1 copy.19
  46.1 0.9 multiply_multiply_fusion
  46.9 0.5 slice_negate_fusion.1
  47.4 1.5 fusion.43
  48.9 0.5 fusion.41
  49.5 0.5 fusion.26
  50.0 1.3 bitcast_reduce_fusion
  51.4 0.0 copy-start.4
  51.4 3.2 copy-done.1
  54.6 1.4 fusion.1
  56.0 0.1 copy.20
  56.1 31.3 %all-gather = bf16[2048,128]{0,1:T(8,128)(2,1)S(1)} all-gather(bf16[256,128]{0,1:T(8,128)(2,1)S(1)} %copy.20), channel_id=2, replica_groups=mesh['sp'=8,'tp'=4] {'sp'}, dimensions={0}, use_global_device_ids=true | all-gather | bytes 589824 | tf_op jit(solution)/shard_map/all_gather | solution.py:74
  87.4 5.1 %fusion.16 = bf16[1,128,256,4]{2,1,3,0:T(8,128)(2,1)S(1)} fusion(f32[2048,256,4]{1,0,2:T(8,128)} %copy-done.1, f32[256,4]{0,1:T(4,128)S(1)} %get-tuple-element.50, bf16[2048,128]{0,1:T(8,128)(2,1)S(1)} %all-gather, f32[256,4]{0,1:T(4,128)S(1)} %get-tuple-element.43, f32[256,4]{0,1:T(4,128)S(1)} %get-tuple-element.42), kind=kOutput, calls=%fused_computation.14 | convolution fusion | flops 543555584 | bytes 9187328 | tf_op jit(solution)/shard_map/while/body/eval_jaxpr/qkgs,skd->qkgd/dot_general | solution.py:93
  92.5 1.7 convolution_convert_fusion
  94.2 0.0 reduce-scatter.3.cloned.1.call-update
  94.2 0.0 all-gather.13.cloned.1.call-start
  94.2 0.5 all-gather.13.cloned.1.call-update
  94.8 0.0 all-gather.7.cloned.1.call-start
  94.8 25.5 %reduce-scatter.3.cloned.1.call-done = bf16[64,2048]{1,0:T(8,128)(2,1)} async-done(((bf16[256,2048]{1,0:T(8,128)(2,1)}), bf16[64,2048]{1,0:T(8,128)(2,1)}) %reduce-scatter.3.cloned.1.call-update) | async-done | bytes 262160 | tf_op jit(solution)/shard_map/reduce_scatter | solution.py:101
  120.4 1.1 fusion.19
  121.5 1.8 fusion.21
  123.3 0.0 all-gather.7.cloned.1.call-update
  123.3 0.0 all-gather.9.cloned.1.call-start
  123.4 0.5 all-gather.9.cloned.1.call-update
  123.9 0.0 all-gather.11.cloned.1.call-start
  124.0 0.7 all-gather.11.cloned.1.call-update
  124.6 0.2 reduce-scatter.5.cloned.1.call-start
  124.9 65.4 %all-gather.13.cloned.1.call-done = bf16[11264,256]{1,0:T(8,128)(2,1)} async-done(((bf16[1408,256]{1,0:T(8,128)(2,1)}), bf16[11264,256]{1,0:T(8,128)(2,1)}) %all-gather.13.cloned.1.call-update) | async-done | bytes 5767184 | tf_op jit(solution)/shard_map/all_gather | solution.py:59
  190.2 8.3 %copy.22 = bf16[1408,8,256]{0,2,1:T(8,128)(2,1)} copy(bf16[1408,8,256]{2,0,1:T(8,128)(2,1)} %bitcast.75) | data formatting | bytes 11534336 | tf_op jit(solution)/shard_map/reshape | solution.py:60
  198.6 7.9 %all-gather.7.cloned.1.call-done = bf16[256,2048]{1,0:T(8,128)(2,1)} async-done(((bf16[64,2048]{1,0:T(8,128)(2,1)}), bf16[256,2048]{1,0:T(8,128)(2,1)}) %all-gather.7.cloned.1.call-update) | async-done | bytes 1048592 | tf_op jit(solution)/shard_map/all_gather | solution.py:112
  206.4 94.2 %all-gather.9.cloned.1.call-done = bf16[2048,1408]{1,0:T(8,128)(2,1)} async-done(((bf16[256,1408]{1,0:T(8,128)(2,1)}), bf16[2048,1408]{1,0:T(8,128)(2,1)}) %all-gather.9.cloned.1.call-update) | async-done | bytes 5767184 | tf_op jit(solution)/shard_map/all_gather | solution.py:56
  300.6 5.9 %fusion.53 = f32[256,1408]{1,0:T(8,128)} fusion(bf16[256,2048]{1,0:T(8,128)(2,1)} %all-gather.7.cloned.1.call-done, bf16[2048,1408]{1,0:T(8,128)(2,1)} %all-gather.9.cloned.1.call-done), kind=kOutput, calls=%fused_computation.88 | convolution fusion | flops 1476395008 | bytes 8257536 | tf_op jit(solution)/shard_map/dot_general | solution.py:113
  306.6 86.6 %all-gather.11.cloned.1.call-done = bf16[2048,1408]{1,0:T(8,128)(2,1)} async-done(((bf16[256,1408]{1,0:T(8,128)(2,1)}), bf16[2048,1408]{1,0:T(8,128)(2,1)}) %all-gather.11.cloned.1.call-update) | async-done | bytes 5767184 | tf_op jit(solution)/shard_map/all_gather | solution.py:57
  393.1 9.5 %convolution_convert_fusion.1 = bf16[256,2048]{1,0:T(8,128)(2,1)} fusion(bf16[1408,2048]{0,1:T(8,128)(2,1)} %bitcast.76, bf16[256,2048]{1,0:T(8,128)(2,1)} %all-gather.7.cloned.1.call-done, bf16[2048,1408]{1,0:T(8,128)(2,1)} %all-gather.11.cloned.1.call-done, f32[256,1408]{1,0:T(8,128)} %fusion.53), kind=kOutput, calls=%fused_computation.10 | convolution fusion | flops 2955476992 | bytes 15073280 | tf_op jit(solution)/shard_map/dot_general | solution.py:116
  402.6 0.0 reduce-scatter.5.cloned.1.call-update
  402.7 23.1 %reduce-scatter.5.cloned.1.call-done = bf16[64,2048]{1,0:T(8,128)(2,1)} async-done(((bf16[256,2048]{1,0:T(8,128)(2,1)}), bf16[64,2048]{1,0:T(8,128)(2,1)}) %reduce-scatter.5.cloned.1.call-update) | async-done | bytes 262160 | tf_op jit(solution)/shard_map/reduce_scatter | solution.py:117
  425.8 1.8 fusion.22
  (15 shorter events, 0.1 us)
Async XLA Ops:
  7.4 85.1 %copy-start = (bf16[512,2048]{1,0:T(8,128)(2,1)S(1)}, bf16[512,2048]{1,0:T(8,128)(2,1)}, u32[]{:S(2)}) copy-start(bf16[512,2048]{1,0:T(8,128)(2,1)} %param.17) | copy-start | bytes 6291460
  7.4 113.0 %reduce-scatter.3.cloned.1.call-start = ((), (), s32[]{:S(2)}) async-start(), calls=%async_computation.2 | async-start | bytes 1310720 | tf_op jit(solution)/shard_map/reduce_scatter | solution.py:101
  51.3 3.2 copy-start.1
  51.4 4.6 %copy-start.4 = (bf16[256,128]{1,0:T(8,128)(2,1)S(1)}, bf16[256,128]{1,0:T(8,128)(2,1)}, u32[]{:S(2)}) copy-start(bf16[256,128]{1,0:T(8,128)(2,1)} %param.14) | copy-start | bytes 196612
  87.4 33.0 %copy-start.2 = (bf16[64,2048]{1,0:T(8,128)(2,1)S(1)}, bf16[64,2048]{1,0:T(8,128)(2,1)}, u32[]{:S(2)}) copy-start(bf16[64,2048]{1,0:T(8,128)(2,1)} %param.11) | copy-start | bytes 786436
  87.4 34.1 %copy-start.5 = (f32[2048]{0:T(1024)S(1)}, f32[2048]{0:T(1024)}, u32[]{:S(2)}) copy-start(f32[2048]{0:T(1024)} %param.18) | copy-start | bytes 24580
  94.2 96.0 %all-gather.13.cloned.1.call-start = ((), (), s32[]{:S(2)}) async-start(), calls=%async_computation.7 | async-start | bytes 6488064 | tf_op jit(solution)/shard_map/all_gather | solution.py:59
  94.8 111.6 %all-gather.7.cloned.1.call-start = ((), (), s32[]{:S(2)}) async-start(), calls=%async_computation.3 | async-start | bytes 1310720 | tf_op jit(solution)/shard_map/all_gather | solution.py:112
  123.3 177.3 %all-gather.9.cloned.1.call-start = ((), (), s32[]{:S(2)}) async-start(), calls=%async_computation.4 | async-start | bytes 6488064 | tf_op jit(solution)/shard_map/all_gather | solution.py:56
  123.9 269.2 %all-gather.11.cloned.1.call-start = ((), (), s32[]{:S(2)}) async-start(), calls=%async_computation.5 | async-start | bytes 6488064 | tf_op jit(solution)/shard_map/all_gather | solution.py:57
  124.6 301.1 %reduce-scatter.5.cloned.1.call-start = ((), (), s32[]{:S(2)}) async-start(), calls=%async_computation.6 | async-start | bytes 1310720 | tf_op jit(solution)/shard_map/reduce_scatter | solution.py:117
  393.1 32.6 %copy-start.3 = (bf16[64,2048]{1,0:T(8,128)(2,1)S(1)}, bf16[64,2048]{1,0:T(8,128)(2,1)}, u32[]{:S(2)}) copy-start(bf16[64,2048]{1,0:T(8,128)(2,1)} %reduce-scatter.3.cloned.1.call-done) | copy-start | bytes 786436
Sparse Core Ops, SparseCore 0:
  94.3 26.0 reduce-scatter.2
  402.8 22.9 reduce-scatter.4
Sparse Core Ops, SparseCore 1:
  96.9 93.3 all-gather.12
  191.7 14.7 all-gather.6
  208.5 92.1 all-gather.8
  302.8 90.2 all-gather.10
